TPU v7x, 32 devices: a whole 2x2x4 slice. The times are simulated.
32 devices in a mesh: fs: 8 (over z, core), tp: 4 (over y, x).
Axes of the slice: x: 2, y: 2, z: 4, core: 2. Of those that a mesh axis runs over, the one named last changes fastest.
Arguments:
- gate_pre: bfloat16 [8192, 5632], P('fs', 'tp'), may hold values from -6 to 6
- up_pre: bfloat16 [8192, 5632], P('fs', 'tp'), may hold values from -6 to 6
- gate_taps: bfloat16 [3, 5632], replicated, may hold values from -3.5 to 3.5
- up_taps: bfloat16 [3, 5632], replicated, may hold values from -3.5 to 3.5
- down_proj: bfloat16 [5632, 2048], P('tp', 'fs'), may hold values from -0.078125 to 0.078125
- cotangent: bfloat16 [8192, 2048], P(('fs', 'tp')), may hold values from -6 to 6
Outputs:
- gate_grad: bfloat16 [8192, 5632], P('fs', 'tp')
- up_grad: bfloat16 [8192, 5632], P('fs', 'tp')
- down_grad: float32 [5632, 2048], P('tp', 'fs')
- row_norms: float32 [5632], P('tp')
- tap_grads: float32 [2, 3, 5632], replicated
All inputs are finite; a program needn't handle non-finite values.
Results may differ from a plain program's by a relative error of at most 0.0042.
Values may be sent and summed in bfloat16 or wider, within the bound.
No kernel may reach another device: no remote copies, remote signals or barrier semaphores. Data moves between devices by JAX's collectives and lax.ppermute only.
A program may use at most 128 MiB of HBM per device.

v0:
```python
import math
import jax
import jax.numpy as jnp
from jax import lax
from jax.sharding import PartitionSpec as P


def from_behind(block, axis, distance):
    devices = range(lax.axis_size(axis))
    route = [(i - distance, i) for i in devices if i - distance in devices]
    return lax.ppermute(block, axis, route)


def body(gate_pre, up_pre, gate_taps, up_taps, down_proj, cotangent):
    row_count = gate_pre.shape[0]
    channels = gate_pre.shape[1]
    tap_count = gate_taps.shape[0]
    reach = tap_count - 1
    channel_start = lax.axis_index("tp") * channels
    gate_taps_f = lax.dynamic_slice_in_dim(gate_taps, channel_start, channels, 1).astype(
        jnp.float32
    )
    up_taps_f = lax.dynamic_slice_in_dim(up_taps, channel_start, channels, 1).astype(jnp.float32)
    before = from_behind((gate_pre[row_count - reach :], up_pre[row_count - reach :]), "fs", 1)
    gate_padded = jnp.concatenate([before[0], gate_pre], axis=0).astype(jnp.float32)
    up_padded = jnp.concatenate([before[1], up_pre], axis=0).astype(jnp.float32)
    gate_conv = gate_taps_f[0] * gate_padded[0:row_count]
    up_conv = up_taps_f[0] * up_padded[0:row_count]
    for offset in range(1, tap_count):
        gate_conv = gate_conv + gate_taps_f[offset] * gate_padded[offset : offset + row_count]
        up_conv = up_conv + up_taps_f[offset] * up_padded[offset : offset + row_count]
    gate_sigmoid = jax.nn.sigmoid(gate_conv)
    gate_act = gate_conv * gate_sigmoid
    hidden = (gate_act * up_conv).astype(jnp.bfloat16)
    whole_cot = lax.all_gather(cotangent, "tp", axis=0, tiled=True)
    cot_cols = whole_cot
    hidden_grad = lax.dot_general(
        cot_cols,
        lax.all_gather(down_proj, "fs", axis=1, tiled=True),
        (((1,), (1,)), ((), ())),
        preferred_element_type=jnp.float32,
    )
    gate_conv_grad = hidden_grad * up_conv * gate_sigmoid * (1.0 + gate_conv * (1.0 - gate_sigmoid))
    up_conv_grad = hidden_grad * gate_act
    following = from_behind((gate_conv_grad[0:reach], up_conv_grad[0:reach]), "fs", -1)
    gate_grad_pad = jnp.concatenate([gate_conv_grad, following[0]], axis=0)
    up_grad_pad = jnp.concatenate([up_conv_grad, following[1]], axis=0)
    gate_grad = gate_taps_f[0] * gate_grad_pad[reach : reach + row_count]
    up_grad = up_taps_f[0] * up_grad_pad[reach : reach + row_count]
    for offset in range(1, tap_count):
        lead = reach - offset
        gate_grad = gate_grad + gate_taps_f[offset] * gate_grad_pad[lead : lead + row_count]
        up_grad = up_grad + up_taps_f[offset] * up_grad_pad[lead : lead + row_count]
    gate_tap_terms = jnp.stack(
        [
            jnp.sum(gate_conv_grad * gate_padded[offset : offset + row_count], axis=0)
            for offset in range(tap_count)
        ]
    )
    up_tap_terms = jnp.stack(
        [
            jnp.sum(up_conv_grad * up_padded[offset : offset + row_count], axis=0)
            for offset in range(tap_count)
        ]
    )
    tap_terms = jnp.stack([gate_tap_terms, up_tap_terms])
    feature_count = whole_cot.shape[1]
    grad_scale = 1.0 / math.sqrt(row_count * lax.axis_size("fs"))
    cot_cols = whole_cot
    own_rows = (
        lax.psum_scatter(
            lax.dot_general(
                cot_cols, hidden, (((0,), (0,)), ((), ())), preferred_element_type=jnp.float32
            ),
            "fs",
            scatter_dimension=0,
            tiled=True,
        )
        * grad_scale
    )
    down_grad = own_rows.T
    partial_norms = jnp.sum(own_rows * own_rows, axis=0)
    norm_sum, tap_sum = lax.psum((partial_norms, tap_terms), "fs")
    row_norms = norm_sum / feature_count
    tap_grads = lax.all_gather(tap_sum * grad_scale, "tp", axis=2, tiled=True)
    return (
        gate_grad.astype(jnp.bfloat16),
        up_grad.astype(jnp.bfloat16),
        down_grad,
        row_norms,
        tap_grads,
    )


def solution(mesh):
    placed = (P("fs", "tp"), P("fs", "tp"), P(), P(), P("tp", "fs"), P(("fs", "tp"), None))
    return jax.shard_map(
        body,
        mesh=mesh,
        in_specs=placed,
        out_specs=(P("fs", "tp"), P("fs", "tp"), P("tp", "fs"), P("tp"), P()),
        check_vma=False,
    )
```

profile of v0, /device:TPU:0, one launch (start us, length us, event | category | flops | bytes accessed | tf_op | source)
XLA Modules:
  0.0 337.2 jit_solution(16197569232840858787)
XLA Ops:
  7.2 0.0 copy-start
  7.2 0.0 all-gather.3.cloned.1.call-start
  7.2 0.7 all-gather.3.cloned.1.call-update
  7.9 0.0 all-gather.5.cloned.1.call-start
  8.0 0.7 all-gather.5.cloned.1.call-update
  8.7 0.0 reduce-scatter.2.cloned.1.call-start
  8.7 0.7 slice.74
  9.5 2.4 collective-permute-start
  11.9 0.7 slice.80
  12.6 4.6 %collective-permute-start.1 = (bf16[2,1408]{1,0:T(2,128)(2,1)S(1)}, bf16[2,1408]{1,0:T(2,128)(2,1)S(1)}, u32[]{:S(2)}, u32[]{:S(2)}) collective-permute-start(bf16[2,1408]{1,0:T(2,128)(2,1)S(1)} %slice.80), channel_id=1, source_target_pairs={{0,4},{4,8},{8,12},{12,16},{16,20},{20,24},{24,28},{1,5},{5,9},{9,... | collective-permute-start | bytes 16904 | tf_op jit(solution)/shard_map/ppermute | solution.py:11
  17.2 0.7 dynamic-slice_convert_fusion
  18.0 0.1 slice_reduce_fusion.5
  18.0 0.0 collective-permute-done
  18.1 5.2 %maximum_convert_fusion = f32[1026,1408]{1,0:T(8,128)} fusion(bf16[1024,1408]{1,0:T(8,128)(2,1)} %param.7, bf16[2,1408]{1,0:T(2,128)(2,1)S(1)} %collective-permute-done), kind=kLoop, calls=%fused_computation.31 | loop fusion | flops 5778432 | bytes 8667648 | tf_op jit(solution)/shard_map/convert_element_type | solution.py:26
  23.2 0.0 collective-permute-done.1
  23.2 0.0 copy-done
  23.2 3.1 maximum_convert_fusion.1
  26.3 38.9 %all-gather.3.cloned.1.call-done = bf16[1024,2048]{1,0:T(8,128)(2,1)} async-done(((bf16[256,2048]{1,0:T(8,128)(2,1)}), bf16[1024,2048]{1,0:T(8,128)(2,1)}) %all-gather.3.cloned.1.call-update) | async-done | bytes 4194320 | tf_op jit(solution)/shard_map/all_gather | solution.py:35
  65.2 62.4 %all-gather.5.cloned.1.call-done = bf16[1408,2048]{1,0:T(8,128)(2,1)} async-done(((bf16[1408,256]{1,0:T(8,128)(2,1)}), bf16[1408,2048]{1,0:T(8,128)(2,1)}) %all-gather.5.cloned.1.call-update) | async-done | bytes 5767184 | tf_op jit(solution)/shard_map/all_gather | solution.py:39
  127.6 32.1 %multiply_reduce_fusion.5 = (f32[1408]{0:T(1024)S(1)}, f32[1408]{0:T(1024)S(1)}, f32[1408]{0:T(1024)S(1)}, f32[1024,1408]{1,0:T(8,128)}, f32[1024,1408]{1,0:T(8,...) fusion(f32[1026,1408]{1,0:T(8,128)} %maximum_convert_fusion.1, f32[1026,1408]{1,0:T(8,128)} %maximum_convert_fusion, ...), kind=kOutput, calls=%fused_computation.24 | convolution fusion | flops 5941620224 | bytes 67683840 | tf_op jit(solution)/shard_map/dot_general | solution.py:37
  159.7 14.2 %convolution_bitcast_fusion = f32[2048,1408]{0,1:T(8,128)} fusion(bf16[1024,2048]{1,0:T(8,128)(2,1)} %all-gather.3.cloned.1.call-done, f32[1024,1408]{1,0:T(8,128)} %get-tuple-element.25, f32[1024,1408]{1,0:T(8,128)} %get-tuple-element.26), kind=kOutput, calls=%fused_computation | convolution fusion | flops 5914230784 | bytes 27262976 | tf_op jit(solution)/shard_map/dot_general | solution.py:72
  173.8 0.0 slice-start
  173.8 0.0 reduce-scatter.2.cloned.1.call-update
  173.9 0.0 slice-start.1
  173.9 12.1 %multiply_reduce_fusion.2 = (f32[1408]{0:T(1024)S(1)}, f32[1408]{0:T(1024)S(1)}, f32[1408]{0:T(1024)S(1)}, f32[1024,1408]{1,0:T(8,128)S(1)}) fusion(f32[1026,1408]{1,0:T(8,128)} %maximum_convert_fusion, f32[1024,1408]{1,0:T(8,128)} %get-tuple-element.30, f32[1024,1408]{1,0:T(8,128)} %get-tuple-element.26), kind=kLoop, calls=%fused_computation.21 | loop fusion | flops 15855488 | bytes 34619904 | tf_op jit(solution)/shard_map/reduce_sum | solution.py:62
  186.1 0.0 slice-done
  186.1 0.0 slice-done.1
  186.2 1.3 collective-permute-start.2
  187.5 1.5 collective-permute-start.3
  189.0 0.2 collective-permute-done.2
  189.2 5.2 %fusion.9 = bf16[1024,1408]{1,0:T(8,128)(2,1)} fusion(f32[1024,1408]{1,0:T(8,128)S(1)} %bitcast.12, f32[2,1408]{1,0:T(2,128)S(1)} %collective-permute-done.2, f32[1408]{0:T(1024)S(1)} %get-tuple-element.20, f32[1408]{0:T(1024)S(1)} %get-tuple-element.21, f32[1408]{0:T(1024)S(1)} %get-tuple-element.19), kind=kLoop, calls=%fused_computation.14 | loop fusion | flops 11534336 | bytes 8678912 | tf_op jit(solution)/shard_map/convert_element_type | solution.py:87
  194.5 0.0 collective-permute-done.3
  194.5 5.3 %fusion.4 = bf16[1024,1408]{1,0:T(8,128)(2,1)} fusion(f32[1024,1408]{1,0:T(8,128)S(1)} %get-tuple-element.27, f32[2,1408]{1,0:T(2,128)S(1)} %collective-permute-done.3, f32[1408]{0:T(1024)S(1)} %get-tuple-element.17, f32[1408]{0:T(1024)S(1)} %get-tuple-element.18, f32[1408]{0:T(1024)S(1)} %get-tuple-element.16), kind=kLoop, calls=%fused_computation.9 | loop fusion | flops 11534336 | bytes 8678912 | tf_op jit(solution)/shard_map/convert_element_type | solution.py:88
  199.8 91.9 %reduce-scatter.2.cloned.1.call-done = f32[256,1408]{0,1:T(8,128)} async-done(((f32[2048,1408]{0,1:T(8,128)}), f32[256,1408]{0,1:T(8,128)}) %reduce-scatter.2.cloned.1.call-update) | async-done | bytes 1441808 | tf_op jit(solution)/shard_map/reduce_scatter | solution.py:71
  291.7 2.6 multiply_reduce_fusion.6
  294.3 26.4 %all-reduce = (f32[1408]{0:T(1024)S(1)}, f32[2,3,1408]{2,1,0:T(4,128)S(1)}) all-reduce(f32[1408]{0:T(1024)S(1)} %get-tuple-element.28, f32[2,3,1408]{2,1,0:T(4,128)S(1)} %pad_maximum_fusion.2), channel_id=1, replica_groups=mesh['fs'=8,'tp'=4] {'fs'}, use_global_device_ids=true, to_apply=%region_2.0 | all-reduce | flops 9856 | bytes 78848 | tf_op jit(solution)/shard_map/psum | solution.py:83
  320.6 0.6 broadcast_multiply_fusion.1
  321.2 8.7 %all_gather.11 = f32[2,3,5632]{2,1,0:T(4,128)S(1)} all-gather(f32[2,3,1408]{2,1,0:T(4,128)S(1)} %broadcast_multiply_fusion), channel_id=1, replica_groups=mesh['fs'=8,'tp'=4] {'tp'}, dimensions={2}, use_global_device_ids=true | all-gather | bytes 168960 | tf_op jit(solution)/shard_map/all_gather | solution.py:85
  329.9 0.7 copy.11
  (14 shorter events, 0.2 us)
Async XLA Ops:
  7.2 16.1 %copy-start = (bf16[1024,1408]{1,0:T(8,128)(2,1)S(1)}, bf16[1024,1408]{1,0:T(8,128)(2,1)}, u32[]{:S(2)}) copy-start(bf16[1024,1408]{1,0:T(8,128)(2,1)} %param.6) | copy-start | bytes 8650756
  7.2 58.0 %all-gather.3.cloned.1.call-start = ((), (), s32[]{:S(2)}) async-start(), calls=%async_computation.1 | async-start | bytes 5242880 | tf_op jit(solution)/shard_map/all_gather | solution.py:35
  7.9 119.7 %all-gather.5.cloned.1.call-start = ((), (), s32[]{:S(2)}) async-start(), calls=%async_computation.2 | async-start | bytes 6488064 | tf_op jit(solution)/shard_map/all_gather | solution.py:39
  8.7 283.0 %reduce-scatter.2.cloned.1.call-start = ((), (), s32[]{:S(2)}) async-start(), calls=%async_computation.3 | async-start | bytes 12976128 | tf_op jit(solution)/shard_map/reduce_scatter | solution.py:71
  9.5 8.6 %collective-permute-start = (bf16[2,1408]{1,0:T(2,128)(2,1)S(1)}, bf16[2,1408]{1,0:T(2,128)(2,1)S(1)}, u32[]{:S(2)}, u32[]{:S(2)}) collective-permute-start(bf16[2,1408]{1,0:T(2,128)(2,1)S(1)} %slice.74), channel_id=1, source_target_pairs={{0,4},{4,8},{8,12},{12,16},{16,20},{20,24},{24,28},{1,5},{5,9},{9,... | collective-permute-start | bytes 16904 | tf_op jit(solution)/shard_map/ppermute | solution.py:11
  12.6 10.6 %collective-permute-start.1 = (bf16[2,1408]{1,0:T(2,128)(2,1)S(1)}, bf16[2,1408]{1,0:T(2,128)(2,1)S(1)}, u32[]{:S(2)}, u32[]{:S(2)}) collective-permute-start(bf16[2,1408]{1,0:T(2,128)(2,1)S(1)} %slice.80), channel_id=1, source_target_pairs={{0,4},{4,8},{8,12},{12,16},{16,20},{20,24},{24,28},{1,5},{5,9},{9,... | collective-permute-start | bytes 16904 | tf_op jit(solution)/shard_map/ppermute | solution.py:11
  173.8 12.3 %slice-start = ((s8[5767168]{0:T(1024)(128)(4,1)}), s8[1572864]{0:T(1024)(128)(4,1)S(1)}, s32[]{:S(2)}) async-start(s8[5767168]{0:T(1024)(128)(4,1)} %bitcast.11), calls=%async_computation.4 | async-start | bytes 3145728
  173.9 12.3 %slice-start.1 = ((s8[5767168]{0:T(1024)(128)(4,1)}), s8[4194304]{0:T(1024)(128)(4,1)S(1)}, s32[]{:S(2)}) async-start(s8[5767168]{0:T(1024)(128)(4,1)} %bitcast.11), calls=%async_computation.5 | async-start | bytes 8388608
  186.2 3.1 collective-permute-start.2
  187.5 7.0 %collective-permute-start.3 = (f32[2,1408]{1,0:T(2,128)S(1)}, f32[2,1408]{1,0:T(2,128)S(1)}, u32[]{:S(2)}, u32[]{:S(2)}) collective-permute-start(f32[2,1408]{1,0:T(2,128)S(1)} %slice.107), channel_id=1, source_target_pairs={{4,0},{8,4},{12,8},{16,12},{20,16},{24,20},{28,24},{5,1},{9,5},{13... | collective-permute-start | bytes 33800 | tf_op jit(solution)/shard_map/ppermute | solution.py:11
Sparse Core Ops, SparseCore 0:
  9.8 55.2 all-gather.2
  66.7 60.7 all-gather.4
  174.0 117.6 reduce-scatter.1
where the time goes:
time: 338 us; the launch traced here: 337 us
  waiting for transfers between devices  195 us (58%)
  matrix products  46.2 us (14%)
  blocking collectives  35 us (10%)
  other arithmetic  34.9 us (10%)
  between operations  14 us (4%)
  starting transfers between devices  9.86 us (3%)
    reduce_scatter x1, waiting for transfers between devices, body(): lax.psum_scatter(lax.dot_general(cot_cols, hidden, (((0,), (0,)), ((), ()...  91.9 us
    all_gather x1, waiting for transfers between devices, body(): lax.all_gather(down_proj, 'fs', axis=1, tiled=True)  62.4 us
    all_gather x1, waiting for transfers between devices, body(): whole_cot = lax.all_gather(cotangent, 'tp', axis=0, tiled=True)  38.9 us
    dot_general x1, matrix products, body(): lax.dot_general(cot_cols, lax.all_gather(down_proj, 'fs', axis=1, tiled=T...  32.1 us
    psum x1, blocking collectives, body(): norm_sum, tap_sum = lax.psum((partial_norms, tap_terms), 'fs')  26.4 us
    dot_general x1, matrix products, body(): lax.dot_general(cot_cols, hidden, (((0,), (0,)), ((), ())), preferred_ele...  14.2 us
    reduce_sum x1, other arithmetic, body(): jnp.sum(up_conv_grad * up_padded[offset:offset + row_count], axis=0)  12.1 us
    ppermute x4, starting transfers between devices, from_behind(): return lax.ppermute(block, axis, route)  9.74 us
  transfers between devices with their start and end apart: 7, of which 4 were waited for; matrix products, arithmetic and copies ran while one was open for 10% of the time, Pallas kernels for 0%

commit v1 on v0

--- a/solution.py
+++ b/solution.py
@@ -1,8 +1,31 @@
+import functools
 import math
 import jax
 import jax.numpy as jnp
 from jax import lax
 from jax.sharding import PartitionSpec as P
+
+
+def _create_limits(values, where_dim):
+    dev_count = lax.axis_size("tp")
+    inbox = []
+    for k0 in range(dev_count):
+        inbox.append((k0, (k0 + 1) % dev_count))
+
+    def _plan_page(w1):
+        if len(w1) == dev_count:
+            return w1
+        local_out = _plan_page([lax.ppermute(w1[0], "tp", inbox), *w1])
+        return local_out
+
+    met_up = jnp.concatenate(_plan_page([values]), axis=where_dim)
+    outcome_arr = jnp.roll(
+        met_up, (lax.axis_index("tp") + 1) * values.shape[where_dim], axis=where_dim
+    )
+    return outcome_arr
+
+
+reach_rates_on_mesh = functools.partial(_create_limits, where_dim=0)
 
 
 def from_behind(block, axis, distance):
@@ -32,7 +55,7 @@
     gate_sigmoid = jax.nn.sigmoid(gate_conv)
     gate_act = gate_conv * gate_sigmoid
     hidden = (gate_act * up_conv).astype(jnp.bfloat16)
-    whole_cot = lax.all_gather(cotangent, "tp", axis=0, tiled=True)
+    whole_cot = reach_rates_on_mesh(cotangent)
     cot_cols = whole_cot
     hidden_grad = lax.dot_general(
         cot_cols,

time: 338 us -> 306 us (0.905)
  waiting for transfers between devices: 195 us -> 152 us
  local copies, waits for them, and re-layouts: 2.38 us -> 12.5 us
    all_gather x1, waiting for transfers between devices: 62.4 us -> 0.01 us  [body(): lax.all_gather(down_proj, 'fs', axis=1, tiled=True)]
    ppermute x0 -> x3, waiting for transfers between devices: none -> 57.5 us  [_plan_page(): local_out = _plan_page([lax.ppermute(w1[0], 'tp', inbox), *w1])]
    all_gather x1 -> x0, waiting for transfers between devices: 38.9 us -> none  [body(): whole_cot = lax.all_gather(cotangent, 'tp', axis=0, tiled=True)]
    unnamed x7 -> x17, local copies, waits for them, and re-layouts: 0.74 us -> 9.78 us
    ppermute x0 -> x3, starting transfers between devices: none -> 3.8 us  [_plan_page(): local_out = _plan_page([lax.ppermute(w1[0], 'tp', inbox), *w1])]
  transfers between devices with their start and end apart: 7 -> 9, of which waited for: 4 -> 5; matrix products, arithmetic and copies ran while one was open for 10% -> 14% of each run, Pallas kernels for 0% -> 0%
where the time goes in v1:
time: 306 us; the launch traced here: 305 us
  waiting for transfers between devices  152 us (50%)
  matrix products  45.7 us (15%)
  blocking collectives  35.1 us (11%)
  other arithmetic  33.5 us (11%)
  between operations  14.3 us (5%)
  local copies, waits for them, and re-layouts  12.5 us (4%)
  starting transfers between devices  12.1 us (4%)
    reduce_scatter x1, waiting for transfers between devices, body(): lax.psum_scatter(lax.dot_general(cot_cols, hidden, (((0,), (0,)), ((), ()...  93.8 us
    ppermute x3, waiting for transfers between devices, _plan_page(): local_out = _plan_page([lax.ppermute(w1[0], 'tp', inbox), *w1])  57.5 us
    dot_general x1, matrix products, body(): lax.dot_general(cot_cols, lax.all_gather(down_proj, 'fs', axis=1, tiled=T...  31 us
    psum x1, blocking collectives, body(): norm_sum, tap_sum = lax.psum((partial_norms, tap_terms), 'fs')  26.4 us
    dot_general x1, matrix products, body(): lax.dot_general(cot_cols, hidden, (((0,), (0,)), ((), ())), preferred_ele...  14.6 us
    reduce_sum x1, other arithmetic, body(): jnp.sum(up_conv_grad * up_padded[offset:offset + row_count], axis=0)  12.1 us
    unnamed x17, local copies, waits for them, and re-layouts  9.78 us
    all_gather x1, blocking collectives, body(): tap_grads = lax.all_gather(tap_sum * grad_scale, 'tp', axis=2, tiled=True)  8.7 us
  transfers between devices with their start and end apart: 9, of which 5 were waited for; matrix products, arithmetic and copies ran while one was open for 14% of the time, Pallas kernels for 0%

profile of v1, /device:TPU:0, one launch (start us, length us, event | category | flops | bytes accessed | tf_op | source)
XLA Modules:
  0.0 305.4 jit_solution(15671896787286628230)
XLA Ops:
  7.2 0.0 all-gather.2.cloned.1.call-start
  7.2 0.7 all-gather.2.cloned.1.call-update
  7.9 0.0 reduce-scatter.2.cloned.1.call-start
  7.9 3.0 collective-permute-start
  11.0 24.3 %collective-permute-done = bf16[256,2048]{1,0:T(8,128)(2,1)S(1)} collective-permute-done((bf16[256,2048]{1,0:T(8,128)(2,1)}, bf16[256,2048]{1,0:T(8,128)(2,1)S(1)}, u32[]{:S(2)}, u32[]{:S(2)}) %collective-permute-start) | collective-permute-done | bytes 1048608 | tf_op jit(solution)/shard_map/ppermute | solution.py:18
  35.3 0.8 collective-permute-start.1
  36.1 0.7 slice.74
  36.8 1.3 collective-permute-start.3
  38.1 0.7 slice.80
  38.9 4.2 %collective-permute-start.4 = (bf16[2,1408]{1,0:T(2,128)(2,1)S(1)}, bf16[2,1408]{1,0:T(2,128)(2,1)S(1)}, u32[]{:S(2)}, u32[]{:S(2)}) collective-permute-start(bf16[2,1408]{1,0:T(2,128)(2,1)S(1)} %slice.80), channel_id=1, source_target_pairs={{0,4},{4,8},{8,12},{12,16},{16,20},{20,24},{24,28},{1,5},{5,9},{9,... | collective-permute-start | bytes 16904 | tf_op jit(solution)/shard_map/ppermute | solution.py:34
  43.1 0.7 dynamic-slice_convert_fusion
  43.9 0.1 slice_reduce_fusion.5
  43.9 0.0 copy-start.1
  44.0 16.7 %collective-permute-done.1 = bf16[256,2048]{1,0:T(8,128)(2,1)S(1)} collective-permute-done((bf16[256,2048]{1,0:T(8,128)(2,1)S(1)}, bf16[256,2048]{1,0:T(8,128)(2,1)S(1)}, u32[]{:S(2)}, u32[]{:S(2)}) %collective-permute-start.1) | collective-permute-done | bytes 1048608 | tf_op jit(solution)/shard_map/ppermute | solution.py:18
  60.6 0.0 collective-permute-start.2
  60.6 0.0 collective-permute-done.3
  60.6 4.9 %maximum_convert_fusion = f32[1026,1408]{1,0:T(8,128)} fusion(bf16[1024,1408]{1,0:T(8,128)(2,1)} %param.7, bf16[2,1408]{1,0:T(2,128)(2,1)S(1)} %collective-permute-done.3), kind=kLoop, calls=%fused_computation.34 | loop fusion | flops 5778432 | bytes 8667648 | tf_op jit(solution)/shard_map/convert_element_type | solution.py:49
  65.5 0.0 collective-permute-done.4
  65.5 0.0 copy-done.1
  65.5 3.1 %maximum_convert_fusion.1 = f32[1026,1408]{1,0:T(8,128)} fusion(bf16[1024,1408]{1,0:T(8,128)(2,1)S(1)} %copy-done.1, bf16[2,1408]{1,0:T(2,128)(2,1)S(1)} %collective-permute-done.4), kind=kLoop, calls=%fused_computation.35 | loop fusion | flops 5778432 | bytes 8667648 | tf_op jit(solution)/shard_map/convert_element_type | solution.py:48
  68.6 16.5 %collective-permute-done.2 = bf16[256,2048]{1,0:T(8,128)(2,1)S(1)} collective-permute-done((bf16[256,2048]{1,0:T(8,128)(2,1)S(1)}, bf16[256,2048]{1,0:T(8,128)(2,1)S(1)}, u32[]{:S(2)}, u32[]{:S(2)}) %collective-permute-start.2) | collective-permute-done | bytes 1048608 | tf_op jit(solution)/shard_map/ppermute | solution.py:18
  85.1 1.1 constant_dynamic-update-slice_fusion.7
  86.2 1.0 constant_dynamic-update-slice_fusion.6
  87.2 1.1 constant_dynamic-update-slice_fusion.5
  88.3 0.0 copy-done
  88.3 1.1 constant_dynamic-update-slice_fusion.4
  89.4 1.1 constant_dynamic-update-slice_fusion.3
  90.5 1.0 constant_dynamic-update-slice_fusion.2
  91.5 1.1 constant_dynamic-update-slice_fusion.1
  92.6 1.1 constant_dynamic-update-slice_fusion
  93.7 31.0 %multiply_reduce_fusion.5 = (f32[1408]{0:T(1024)S(1)}, f32[1408]{0:T(1024)S(1)}, f32[1408]{0:T(1024)S(1)}, f32[1024,1408]{1,0:T(8,128)}, f32[1024,1408]{1,0:T(8,...) fusion(f32[1026,1408]{1,0:T(8,128)} %maximum_convert_fusion.1, f32[1026,1408]{1,0:T(8,128)} %maximum_convert_fusion, ...), kind=kOutput, calls=%fused_computation.23 | convolution fusion | flops 5941620224 | bytes 67683840 | tf_op jit(solution)/shard_map/dot_general | solution.py:60
  124.7 14.6 %fusion.13 = f32[2048,1408]{1,0:T(8,128)} fusion(bf16[2048,2048]{1,0:T(8,128)(2,1)} %constant_dynamic-update-slice_fusion, s32[]{:T(128)S(6)} %select_n.19, f32[1024,1408]{1,0:T(8,128)} %get-tuple-element.30, f32[1024,1408]{1,0:T(8,128)} %get-tuple-element.31), kind=kOutput, calls=%fused_computation.30 | convolution fusion | flops 5914230784 | bytes 27262980 | tf_op jit(solution)/shard_map/dot_general | solution.py:95
  139.3 0.0 reduce-scatter.2.cloned.1.call-update
  139.3 0.0 slice-start.1
  139.4 12.1 %multiply_reduce_fusion.2 = (f32[1408]{0:T(1024)S(1)}, f32[1408]{0:T(1024)S(1)}, f32[1408]{0:T(1024)S(1)}, f32[1024,1408]{1,0:T(8,128)S(1)}) fusion(f32[1026,1408]{1,0:T(8,128)} %maximum_convert_fusion, f32[1024,1408]{1,0:T(8,128)} %get-tuple-element.35, f32[1024,1408]{1,0:T(8,128)} %get-tuple-element.31), kind=kLoop, calls=%fused_computation.20 | loop fusion | flops 15855488 | bytes 34619904 | tf_op jit(solution)/shard_map/reduce_sum | solution.py:85
  151.6 1.3 collective-permute-start.5
  152.9 1.5 collective-permute-start.6
  154.5 0.2 collective-permute-done.5
  154.7 5.2 %fusion.9 = bf16[1024,1408]{1,0:T(8,128)(2,1)} fusion(f32[1024,1408]{1,0:T(8,128)S(1)} %bitcast.8, f32[2,1408]{1,0:T(2,128)S(1)} %collective-permute-done.5, f32[1408]{0:T(1024)S(1)} %get-tuple-element.25, f32[1408]{0:T(1024)S(1)} %get-tuple-element.26, f32[1408]{0:T(1024)S(1)} %get-tuple-element.24), kind=kLoop, calls=%fused_computation.13 | loop fusion | flops 11534336 | bytes 8678912 | tf_op jit(solution)/shard_map/convert_element_type | solution.py:110
  159.9 0.0 collective-permute-done.6
  159.9 5.3 %fusion.4 = bf16[1024,1408]{1,0:T(8,128)(2,1)} fusion(f32[1024,1408]{1,0:T(8,128)S(1)} %get-tuple-element.32, f32[2,1408]{1,0:T(2,128)S(1)} %collective-permute-done.6, f32[1408]{0:T(1024)S(1)} %get-tuple-element.22, f32[1408]{0:T(1024)S(1)} %get-tuple-element.23, f32[1408]{0:T(1024)S(1)} %get-tuple-element.21), kind=kLoop, calls=%fused_computation.8 | loop fusion | flops 11534336 | bytes 8678912 | tf_op jit(solution)/shard_map/convert_element_type | solution.py:111
  165.2 93.8 %reduce-scatter.2.cloned.1.call-done = f32[256,1408]{1,0:T(8,128)} async-done(((f32[2048,1408]{1,0:T(8,128)}), f32[256,1408]{1,0:T(8,128)}) %reduce-scatter.2.cloned.1.call-update) | async-done | bytes 1441808 | tf_op jit(solution)/shard_map/reduce_scatter | solution.py:94
  259.0 1.5 multiply_reduce_fusion.6
  260.6 26.4 %all-reduce = (f32[1408]{0:T(1024)S(1)}, f32[2,3,1408]{2,1,0:T(4,128)S(1)}) all-reduce(f32[1408]{0:T(1024)S(1)} %get-tuple-element.33, f32[2,3,1408]{2,1,0:T(4,128)S(1)} %pad_maximum_fusion.2), channel_id=1, replica_groups=mesh['fs'=8,'tp'=4] {'fs'}, use_global_device_ids=true, to_apply=%region_2.3 | all-reduce | flops 9856 | bytes 78848 | tf_op jit(solution)/shard_map/psum | solution.py:106
  286.9 0.6 broadcast_multiply_fusion.1
  287.6 8.7 %all_gather.7 = f32[2,3,5632]{2,1,0:T(4,128)S(1)} all-gather(f32[2,3,1408]{2,1,0:T(4,128)S(1)} %broadcast_multiply_fusion), channel_id=1, replica_groups=mesh['fs'=8,'tp'=4] {'tp'}, dimensions={2}, use_global_device_ids=true | all-gather | bytes 168960 | tf_op jit(solution)/shard_map/all_gather | solution.py:108
  296.3 0.7 copy.13
  297.0 1.5 copy.12
  (19 shorter events, 0.2 us)
Async XLA Ops:
  7.2 86.5 %all-gather.2.cloned.1.call-start = ((), (), s32[]{:S(2)}) async-start(), calls=%async_computation.1 | async-start | bytes 6488064 | tf_op jit(solution)/shard_map/all_gather | solution.py:62
  7.9 251.1 %reduce-scatter.2.cloned.1.call-start = ((), (), s32[]{:S(2)}) async-start(), calls=%async_computation.2 | async-start | bytes 12976128 | tf_op jit(solution)/shard_map/reduce_scatter | solution.py:94
  7.9 27.3 %collective-permute-start = (bf16[256,2048]{1,0:T(8,128)(2,1)}, bf16[256,2048]{1,0:T(8,128)(2,1)S(1)}, u32[]{:S(2)}, u32[]{:S(2)}) collective-permute-start(bf16[256,2048]{1,0:T(8,128)(2,1)} %param.11), channel_id=1, source_target_pairs={{0,1},{1,2},{2,3},{3,0},{4,5},{5,6},{6,7},{7,4},{8,9},{9,10},{10,1... | collective-permute-start | bytes 3145736 | tf_op jit(solution)/shard_map/ppermute | solution.py:18
  35.3 25.3 %collective-permute-start.1 = (bf16[256,2048]{1,0:T(8,128)(2,1)S(1)}, bf16[256,2048]{1,0:T(8,128)(2,1)S(1)}, u32[]{:S(2)}, u32[]{:S(2)}) collective-permute-start(bf16[256,2048]{1,0:T(8,128)(2,1)S(1)} %collective-permute-done), channel_id=1, source_target_pairs={{0,1},{1,2},{2,3},{3,0},{4,5},{5,6},{6,7},{7,4},{8,9},{9,10},{10,1... | collective-permute-start | bytes 3145736 | tf_op jit(solution)/shard_map/ppermute | solution.py:18
  36.8 23.8 %collective-permute-start.3 = (bf16[2,1408]{1,0:T(2,128)(2,1)S(1)}, bf16[2,1408]{1,0:T(2,128)(2,1)S(1)}, u32[]{:S(2)}, u32[]{:S(2)}) collective-permute-start(bf16[2,1408]{1,0:T(2,128)(2,1)S(1)} %slice.74), channel_id=1, source_target_pairs={{0,4},{4,8},{8,12},{12,16},{16,20},{20,24},{24,28},{1,5},{5,9},{9,... | collective-permute-start | bytes 16904 | tf_op jit(solution)/shard_map/ppermute | solution.py:34
  38.9 26.6 %collective-permute-start.4 = (bf16[2,1408]{1,0:T(2,128)(2,1)S(1)}, bf16[2,1408]{1,0:T(2,128)(2,1)S(1)}, u32[]{:S(2)}, u32[]{:S(2)}) collective-permute-start(bf16[2,1408]{1,0:T(2,128)(2,1)S(1)} %slice.80), channel_id=1, source_target_pairs={{0,4},{4,8},{8,12},{12,16},{16,20},{20,24},{24,28},{1,5},{5,9},{9,... | collective-permute-start | bytes 16904 | tf_op jit(solution)/shard_map/ppermute | solution.py:34
  43.9 21.6 %copy-start.1 = (bf16[1024,1408]{1,0:T(8,128)(2,1)S(1)}, bf16[1024,1408]{1,0:T(8,128)(2,1)}, u32[]{:S(2)}) copy-start(bf16[1024,1408]{1,0:T(8,128)(2,1)} %param.6) | copy-start | bytes 8650756
  60.6 24.5 %collective-permute-start.2 = (bf16[256,2048]{1,0:T(8,128)(2,1)S(1)}, bf16[256,2048]{1,0:T(8,128)(2,1)S(1)}, u32[]{:S(2)}, u32[]{:S(2)}) collective-permute-start(bf16[256,2048]{1,0:T(8,128)(2,1)S(1)} %collective-permute-done.1), channel_id=1, source_target_pairs={{0,1},{1,2},{2,3},{3,0},{4,5},{5,6},{6,7},{7,4},{8,9},{9,10},{10,1... | collective-permute-start | bytes 3145736 | tf_op jit(solution)/shard_map/ppermute | solution.py:18
  65.5 22.8 %copy-start = (bf16[256,2048]{1,0:T(8,128)(2,1)S(1)}, bf16[256,2048]{1,0:T(8,128)(2,1)}, u32[]{:S(2)}) copy-start(bf16[256,2048]{1,0:T(8,128)(2,1)} %param.11) | copy-start | bytes 3145732
  139.3 12.2 %slice-start = ((s8[5767168]{0:T(1024)(128)(4,1)}), s8[1572864]{0:T(1024)(128)(4,1)S(1)}, s32[]{:S(2)}) async-start(s8[5767168]{0:T(1024)(128)(4,1)} %bitcast.7), calls=%async_computation.3 | async-start | bytes 3145728
  139.3 12.2 %slice-start.1 = ((s8[5767168]{0:T(1024)(128)(4,1)}), s8[4194304]{0:T(1024)(128)(4,1)S(1)}, s32[]{:S(2)}) async-start(s8[5767168]{0:T(1024)(128)(4,1)} %bitcast.7), calls=%async_computation.4 | async-start | bytes 8388608
  151.6 3.1 %collective-permute-start.5 = (f32[2,1408]{1,0:T(2,128)S(1)}, f32[2,1408]{1,0:T(2,128)S(1)}, u32[]{:S(2)}, u32[]{:S(2)}) collective-permute-start(f32[2,1408]{1,0:T(2,128)S(1)} %slice.104), channel_id=1, source_target_pairs={{4,0},{8,4},{12,8},{16,12},{20,16},{24,20},{28,24},{5,1},{9,5},{13... | collective-permute-start | bytes 33800 | tf_op jit(solution)/shard_map/ppermute | solution.py:34
  152.9 7.0 %collective-permute-start.6 = (f32[2,1408]{1,0:T(2,128)S(1)}, f32[2,1408]{1,0:T(2,128)S(1)}, u32[]{:S(2)}, u32[]{:S(2)}) collective-permute-start(f32[2,1408]{1,0:T(2,128)S(1)} %slice.107), channel_id=1, source_target_pairs={{4,0},{8,4},{12,8},{16,12},{20,16},{24,20},{28,24},{5,1},{9,5},{13... | collective-permute-start | bytes 33800 | tf_op jit(solution)/shard_map/ppermute | solution.py:34
Sparse Core Ops, SparseCore 0:
  9.6 63.5 all-gather.1
  139.5 119.5 reduce-scatter.1
